TPU v7x, 32 devices: a whole 2x2x4 slice. The times are simulated.
32 devices in a mesh: sp: 8 (over z, y), tp: 4 (over x, core).
Axes of the slice: x: 2, y: 2, z: 4, core: 2. Of those that a mesh axis runs over, the one named last changes fastest.
Arguments:
- out_grad: bfloat16 [1024, 2048], P('sp'), may hold values from -6 to 6
- residual: bfloat16 [1024, 2048], P('sp'), may hold values from -6 to 6
- routes: int32 [1024, 2], P('sp'), may hold values from 0 to 3, all different within a row; in each aligned block of 128 rows (0 to 127, 128 to 255, ...) at most 80 rows name the same one
- route_weights: float32 [1024, 2], P('sp'), may hold values from 0.15 to 0.85, as said below
- w_gate: bfloat16 [8, 2048, 2048], P('sp', None, 'tp'), may hold values from -0.125 to 0.125
- w_up: bfloat16 [8, 2048, 2048], P('sp', None, 'tp'), may hold values from -0.125 to 0.125
- w_down: bfloat16 [8, 2048, 2048], P('sp', 'tp'), may hold values from -0.09375 to 0.09375
- out_gate: bfloat16 [1024, 1024], P('sp', 'tp'), may hold values from -6 to 6
- in_gate: bfloat16 [1024, 1024], P('sp', 'tp'), may hold values from -6 to 6
- conv_input: bfloat16 [1024, 1024], P('sp', 'tp'), may hold values from -6 to 6
- conv_out: bfloat16 [1024, 1024], P('sp', 'tp'), may hold values from -6 to 6
- conv_taps: float32 [3, 1024], P(None, 'tp'), may hold values from -3.5 to 3.5
- w_out: bfloat16 [1024, 2048], P('tp'), may hold values from -0.1875 to 0.1875
Outputs:
- grad_resid: bfloat16 [1024, 2048], P('sp')
- grad_up: bfloat16 [8, 2048, 2048], P('sp', None, 'tp')
- grad_down: bfloat16 [8, 2048, 2048], P('sp', 'tp')
- grad_out_gate: bfloat16 [1024, 1024], P('sp', 'tp')
- grad_in_gate: bfloat16 [1024, 1024], P('sp', 'tp')
- grad_conv_input: bfloat16 [1024, 1024], P('sp', 'tp')
- grad_w_out: float32 [2048, 1024], P('sp', 'tp')
Inputs may be any that keep to these rules, and one draw needn't show every extreme that they name: `routes`: each row names 2 different experts. In the rows of one index of sp no expert is named more than 80 times, a bound that some block reaches. `route_weights`: the two weights of a row sum to one.
All inputs are finite; a program needn't handle non-finite values.
Results may differ from a plain program's by a relative error of at most 0.013.
Values may be sent and summed in bfloat16 or wider, within the bound.
A program may use at most 128 MiB of HBM per device.

v0:
```python
import jax
import jax.numpy as jnp
from jax import lax
from jax.sharding import PartitionSpec as P

epsilon = 1e-06


def with_halo(cells, sides, width):
    for axis, dim in sides:
        count = lax.axis_size(axis)
        ends = count - 1
        head = lax.slice_in_dim(cells, 0, width, axis=dim)
        tail = lax.slice_in_dim(cells, cells.shape[dim] - width, cells.shape[dim], axis=dim)
        cells = jnp.concatenate(
            [
                lax.ppermute(tail, axis, [(i, (i + 1) % count) for i in range(ends)]),
                cells,
                lax.ppermute(head, axis, [((i + 1) % count, i) for i in range(ends)]),
            ],
            axis=dim,
        )
    return cells


def per_device(
    out_grad,
    residual,
    routes,
    route_weights,
    w_gate,
    w_up,
    w_down,
    out_gate,
    in_gate,
    conv_input,
    conv_out,
    conv_taps,
    w_out,
):
    tok_rows = out_grad.shape[0]
    features = out_grad.shape[1]
    top_count = routes.shape[1]
    slices = lax.axis_size("sp")
    experts = slices // 2
    capacity = 5 * tok_rows // slices
    n_assign = tok_rows * top_count
    resid_f32 = residual.astype(jnp.float32)
    inv_rms = lax.rsqrt(jnp.mean(resid_f32 * resid_f32, axis=-1, keepdims=True) + epsilon)
    unit_rows = resid_f32 * inv_rms
    normed = unit_rows.astype(jnp.bfloat16)
    weighted = (
        (route_weights[:, :, None] * out_grad.astype(jnp.float32)[:, None, :])
        .astype(jnp.bfloat16)
        .reshape(n_assign, features)
    )
    flat_routes = routes.reshape(-1)
    onehot = (flat_routes[:, None] == jnp.arange(experts, dtype=jnp.int32)[None, :]).astype(
        jnp.int32
    )
    slot_rank = jnp.sum((jnp.cumsum(onehot, axis=0) - onehot) * onehot, axis=1)
    slot_index = flat_routes * capacity + slot_rank
    slot_table = (
        jnp.full((experts * capacity,), n_assign, jnp.int32)
        .at[slot_index]
        .set(jnp.arange(n_assign, dtype=jnp.int32))
    )
    filled = slot_table < n_assign
    safe_index = jnp.where(filled, slot_table, 0)
    send_rows = jnp.where(
        filled[:, None], normed[safe_index // top_count], jnp.zeros((), jnp.bfloat16)
    )
    send_grads = jnp.where(filled[:, None], weighted[safe_index], jnp.zeros((), jnp.bfloat16))
    outgoing = jnp.stack([send_rows, send_grads])
    doubled = jnp.repeat(outgoing.reshape(2, experts, capacity, features), 2, axis=1)
    arrived = lax.all_to_all(doubled, "sp", split_axis=1, concat_axis=1, tiled=True)
    expert_rows = arrived[0].reshape(slices * capacity, features)
    expert_grads = arrived[1].reshape(slices * capacity, features)
    gate_local = w_gate[0]
    up_local = w_up[0]
    down_local = w_down[0]
    pre_gate = jnp.dot(expert_rows, gate_local, preferred_element_type=jnp.float32)
    pre_up = jnp.dot(expert_rows, up_local, preferred_element_type=jnp.float32)
    sigmoid_gate = jax.nn.sigmoid(pre_gate)
    activated = pre_gate * sigmoid_gate
    hidden = (activated * pre_up).astype(jnp.bfloat16)
    d_hidden = lax.dot_general(
        expert_grads, down_local, (((1,), (1,)), ((), ())), preferred_element_type=jnp.float32
    )
    grad_down = lax.dot_general(
        hidden, expert_grads, (((0,), (0,)), ((), ())), preferred_element_type=jnp.float32
    ).astype(jnp.bfloat16)
    d_gate = (d_hidden * pre_up * sigmoid_gate * (1.0 + pre_gate * (1.0 - sigmoid_gate))).astype(
        jnp.bfloat16
    )
    d_up = (d_hidden * activated).astype(jnp.bfloat16)
    grad_up = lax.dot_general(
        expert_rows, d_up, (((0,), (0,)), ((), ())), preferred_element_type=jnp.float32
    ).astype(jnp.bfloat16)
    partial_value = lax.dot_general(
        d_gate, gate_local, (((1,), (1,)), ((), ())), preferred_element_type=jnp.float32
    )
    partial_value = partial_value + lax.dot_general(
        d_up, up_local, (((1,), (1,)), ((), ())), preferred_element_type=jnp.float32
    )
    partial_value = partial_value.astype(jnp.bfloat16).reshape(slices, capacity, features)
    summed = lax.psum_scatter(partial_value, "tp", scatter_dimension=2, tiled=True).astype(
        jnp.float32
    )
    returned = lax.all_to_all(
        summed.astype(jnp.bfloat16), "sp", split_axis=0, concat_axis=0, tiled=True
    )
    columns = returned.shape[2]
    flat_back = returned.reshape(slices * capacity, columns)
    first_index = 2 * flat_routes * capacity + slot_rank
    contrib = flat_back[first_index].astype(jnp.float32) + flat_back[first_index + capacity].astype(
        jnp.float32
    )
    d_normed = jnp.sum(contrib.reshape(tok_rows, top_count, columns), axis=1)
    col_start = lax.axis_index("tp") * columns
    unit_part = lax.dynamic_slice_in_dim(unit_rows, col_start, columns, 1)
    grad_part = lax.dynamic_slice_in_dim(out_grad, col_start, columns, 1).astype(jnp.float32)
    row_dots = lax.psum(jnp.sum(unit_part * d_normed, axis=-1), "tp")
    row_mean = row_dots[:, None] / features
    resid_part = (grad_part + inv_rms * (d_normed - unit_part * row_mean)).astype(jnp.bfloat16)
    grad_resid = lax.all_gather(resid_part, "tp", axis=1, tiled=True)
    d_mix = lax.dot_general(
        grad_resid, w_out, (((1,), (1,)), ((), ())), preferred_element_type=jnp.float32
    )
    conv_f32 = conv_out.astype(jnp.float32)
    gate_f32 = out_gate.astype(jnp.float32)
    grad_out_gate = (d_mix * conv_f32).astype(jnp.bfloat16)
    d_conv = d_mix * gate_f32
    padded = with_halo(d_conv.astype(jnp.bfloat16), (("sp", 0),), 1).astype(d_conv.dtype)
    d_inner = conv_taps[0] * padded[2:] + conv_taps[1] * padded[1:-1] + conv_taps[2] * padded[:-2]
    grad_in_gate = (d_inner * conv_input.astype(jnp.float32)).astype(jnp.bfloat16)
    grad_conv_input = (d_inner * in_gate.astype(jnp.float32)).astype(jnp.bfloat16)
    mixed = (gate_f32 * conv_f32).astype(jnp.bfloat16)
    grad_w_out = lax.psum_scatter(
        lax.dot_general(
            grad_resid, mixed, (((0,), (0,)), ((), ())), preferred_element_type=jnp.float32
        ),
        "sp",
        scatter_dimension=0,
        tiled=True,
    )
    return (
        grad_resid,
        grad_up[None],
        grad_down[None],
        grad_out_gate,
        grad_in_gate,
        grad_conv_input,
        grad_w_out,
    )


def solution(mesh):
    in_specs = (
        P("sp", None),
        P("sp", None),
        P("sp", None),
        P("sp", None),
        P("sp", None, "tp"),
        P("sp", None, "tp"),
        P("sp", "tp", None),
        P("sp", "tp"),
        P("sp", "tp"),
        P("sp", "tp"),
        P("sp", "tp"),
        P(None, "tp"),
        P("tp", None),
    )
    out_specs = (
        P("sp", None),
        P("sp", None, "tp"),
        P("sp", "tp", None),
        P("sp", "tp"),
        P("sp", "tp"),
        P("sp", "tp"),
        P("sp", "tp"),
    )
    return jax.shard_map(
        per_device, mesh=mesh, in_specs=in_specs, out_specs=out_specs, check_vma=False
    )
```

profile of v0, /device:TPU:0, one launch (start us, length us, event | category | flops | bytes accessed | tf_op | source)
XLA Modules:
  0.0 325.3 jit_solution(2175908563554208962)
XLA Ops:
  9.4 1.2 reduce-window.6
  11.4 1.4 scatter_custom_fusion
  12.8 1.2 fusion.12
  15.1 2.2 convert_multiply_fusion
  17.2 2.4 mul.164
  19.6 3.6 %mul.165 = f32[256,2048]{1,0:T(8,128)} reshape(f32[128,2,2048]{2,1,0:T(2,128)} %mul.164) | data formatting | bytes 4194304 | tf_op jit(solution)/shard_map/mul | solution.py:53
  23.3 3.0 gather_fusion
  26.3 1.8 multiply_convert_fusion
  28.1 3.0 gather_fusion.1
  31.1 1.9 broadcast_select_fusion.1
  34.2 122.8 %all_to_all.10 = bf16[2,8,80,2048]{3,2,0,1:T(8,128)(2,1)S(1)} all-to-all(bf16[2,8,80,2048]{3,2,0,1:T(8,128)(2,1)S(1)} %bitcast.65), channel_id=1, replica_groups=mesh['sp'=8,'tp'=4] {'sp'}, dimensions={1} | all-to-all | bytes 10485760 | tf_op jit(solution)/shard_map/all_to_all | solution.py:76
  157.4 1.5 fusion.4
  159.0 1.6 copy-done.5
  160.6 1.5 fusion.7
  162.7 1.7 multiply_convert_fusion.2
  164.4 1.9 fusion.2
  166.3 3.0 add_convert_fusion
  169.4 33.5 %reduce-scatter.3.cloned.1.call-done = bf16[8,80,512]{2,1,0:T(8,128)(2,1)} async-done(((bf16[8,80,2048]{2,1,0:T(8,128)(2,1)}), bf16[8,80,512]{2,1,0:T(8,128)(2,1)}) %reduce-scatter.3.cloned.1.call-update) | async-done | bytes 655376 | tf_op jit(solution)/shard_map/reduce_scatter | solution.py:107
  202.9 5.5 %all-to-all-start.1 = ((bf16[8,80,512]{2,1,0:T(8,128)(2,1)}), bf16[8,80,512]{2,1,0:T(8,128)(2,1)S(1)}, u32[]{:S(2)}, u32[]{:S(2)}) async-start(bf16[8,80,512]{2,1,0:T(8,128)(2,1)} %reduce-scatter.3.cloned.1.call-done), calls=%async_computation.2 | async-start | bytes 1310720 | tf_op jit(solution)/shard_map/all_to_all | solution.py:110
  208.5 17.1 %all-to-all-done.1 = bf16[8,80,512]{2,1,0:T(8,128)(2,1)S(1)} async-done(((bf16[8,80,512]{2,1,0:T(8,128)(2,1)}), bf16[8,80,512]{2,1,0:T(8,128)(2,1)S(1)}, u32[]{:S(2)}, u32[]{:S(2)}) %all-to-all-start.1) | async-done | bytes 655392 | tf_op jit(solution)/shard_map/all_to_all | solution.py:110
  226.7 1.9 gather_fusion.2
  228.6 1.9 convert_add_fusion
  230.5 2.2 add.145
  232.7 1.7 reduce_sum.41
  234.5 5.9 %psum.7 = f32[128]{0:T(128)S(1)} all-reduce(f32[128]{0:T(128)S(1)} %multiply_reduce_fusion), channel_id=1, replica_groups=mesh['sp'=8,'tp'=4] {'tp'}, use_global_device_ids=true, to_apply=%region_8.9 | all-reduce | flops 128 | bytes 1024 | tf_op jit(solution)/shard_map/psum | solution.py:123
  241.4 6.8 %all_gather.3 = bf16[128,2048]{1,0:T(8,128)(2,1)S(1)} all-gather(bf16[128,512]{1,0:T(8,128)(2,1)S(1)} %add_convert_fusion.1), channel_id=1, replica_groups=mesh['sp'=8,'tp'=4] {'tp'}, dimensions={1}, use_global_device_ids=true | all-gather | bytes 655360 | tf_op jit(solution)/shard_map/all_gather | solution.py:126
  248.2 1.8 fusion.20
  250.1 5.9 %fusion.1 = bf16[1,512,2048]{2,1,0:T(8,128)(2,1)} fusion(bf16[640,2048]{1,0:T(8,128)(2,1)} %bitcast.73, f32[640,512]{1,0:T(8,128)} %copy-done.17, f32[640,512]{1,0:T(8,128)} %copy-done.16), kind=kOutput, calls=%fused_computation.9 | convolution fusion | flops 1345191936 | bytes 7340032 | tf_op jit(solution)/shard_map/dot_general | solution.py:90
  257.1 3.4 %collective-permute-start = (bf16[1,256]{1,0:T(2,128)(2,1)S(1)}, bf16[1,256]{1,0:T(2,128)(2,1)S(1)}, u32[]{:S(2)}, u32[]{:S(2)}) collective-permute-start(bf16[1,256]{1,0:T(2,128)(2,1)S(1)} %get-tuple-element.15), channel_id=1, source_target_pairs={{0,4},{4,8},{8,12},{12,16},{16,20},{20,24},{24,28},{1,5},{5,9},{9,... | collective-permute-start | bytes 1544 | tf_op jit(solution)/shard_map/ppermute | solution.py:17
  260.5 1.4 collective-permute-start.1
  262.0 3.2 fusion
  267.5 50.2 %reduce-scatter.5.cloned.1.call-done = f32[256,256]{1,0:T(8,128)} async-done(((f32[2048,256]{1,0:T(8,128)}), f32[256,256]{1,0:T(8,128)}) %reduce-scatter.5.cloned.1.call-update) | async-done | bytes 262160 | tf_op jit(solution)/shard_map/reduce_scatter | solution.py:139
  (83 shorter events, 12.8 us)
Async XLA Ops:
  7.2 150.3 %copy-start = (bf16[1,2048,512]{2,1,0:T(8,128)(2,1)S(1)}, bf16[1,2048,512]{2,1,0:T(8,128)(2,1)}, u32[]{:S(2)}) copy-start(bf16[1,2048,512]{2,1,0:T(8,128)(2,1)} %param.17) | copy-start | bytes 6291460
  7.2 10.1 %copy-start.7 = (bf16[128,2048]{1,0:T(8,128)(2,1)S(1)}, bf16[128,2048]{1,0:T(8,128)(2,1)}, u32[]{:S(2)}) copy-start(bf16[128,2048]{1,0:T(8,128)(2,1)} %param.13) | copy-start | bytes 1572868
  7.2 195.7 %reduce-scatter.3.cloned.1.call-start = ((), (), s32[]{:S(2)}) async-start(), calls=%async_computation.4 | async-start | bytes 3276800 | tf_op jit(solution)/shard_map/reduce_scatter | solution.py:107
  157.4 1.6 copy-start.1
  157.4 4.7 %copy-start.3 = (bf16[1,8,80,2048]{3,2,0,1:T(8,128)(2,1)}, bf16[1,8,80,2048]{3,2,0,1:T(8,128)(2,1)S(1)}, u32[]{:S(2)}) copy-start(bf16[1,8,80,2048]{3,2,0,1:T(8,128)(2,1)S(1)} %get-tuple-element.9) | copy-start | bytes 7864324
  157.4 3.2 copy-start.5
  160.6 3.8 %copy-start.16 = (f32[640,512]{1,0:T(8,128)}, f32[640,512]{1,0:T(8,128)S(1)}, u32[]{:S(2)}) copy-start(f32[640,512]{1,0:T(8,128)S(1)} %fusion.4) | copy-start | bytes 3932164
  160.6 2.1 copy-start.15
  162.1 2.3 copy-start.17
  164.4 2.0 copy-start.8
  202.9 22.7 %all-to-all-start.1 = ((bf16[8,80,512]{2,1,0:T(8,128)(2,1)}), bf16[8,80,512]{2,1,0:T(8,128)(2,1)S(1)}, u32[]{:S(2)}, u32[]{:S(2)}) async-start(bf16[8,80,512]{2,1,0:T(8,128)(2,1)} %reduce-scatter.3.cloned.1.call-done), calls=%async_computation.2 | async-start | bytes 1310720 | tf_op jit(solution)/shard_map/all_to_all | solution.py:110
  208.5 109.2 %reduce-scatter.5.cloned.1.call-start = ((), (), s32[]{:S(2)}) async-start(), calls=%async_computation.5 | async-start | bytes 2359296 | tf_op jit(solution)/shard_map/reduce_scatter | solution.py:139
  228.6 5.8 %copy-start.4 = (f32[128,2048]{1,0:T(8,128)S(1)}, f32[128,2048]{1,0:T(8,128)}, u32[]{:S(2)}) copy-start(f32[128,2048]{1,0:T(8,128)} %get-tuple-element.11) | copy-start | bytes 3145732
  230.5 17.7 %copy-start.10 = (bf16[128,256]{1,0:T(8,128)(2,1)S(1)}, bf16[128,256]{1,0:T(8,128)(2,1)}, u32[]{:S(2)}) copy-start(bf16[128,256]{1,0:T(8,128)(2,1)} %param.20) | copy-start | bytes 196612
  230.5 17.7 %copy-start.11 = (bf16[128,256]{1,0:T(8,128)(2,1)S(1)}, bf16[128,256]{1,0:T(8,128)(2,1)}, u32[]{:S(2)}) copy-start(bf16[128,256]{1,0:T(8,128)(2,1)} %param.23) | copy-start | bytes 196612
  248.2 1.8 copy-start.14
  250.1 5.9 %copy-start.6 = (bf16[256,2048]{1,0:T(8,128)(2,1)S(1)}, bf16[256,2048]{1,0:T(8,128)(2,1)}, u32[]{:S(2)}) copy-start(bf16[256,2048]{1,0:T(8,128)(2,1)} %param.25) | copy-start | bytes 3145732
  250.1 11.9 %copy-start.2 = (bf16[1,8,80,2048]{3,2,0,1:T(8,128)(2,1)S(1)}, bf16[1,8,80,2048]{3,2,0,1:T(8,128)(2,1)}, u32[]{:S(2)}) copy-start(bf16[1,8,80,2048]{3,2,0,1:T(8,128)(2,1)} %copy-done.1) | copy-start | bytes 7864324
  250.1 11.9 %copy-start.9 = (bf16[640,512]{1,0:T(8,128)(2,1)S(1)}, bf16[640,512]{1,0:T(8,128)(2,1)}, u32[]{:S(2)}) copy-start(bf16[640,512]{1,0:T(8,128)(2,1)} %copy-done.8) | copy-start | bytes 1966084
  257.1 8.0 %collective-permute-start = (bf16[1,256]{1,0:T(2,128)(2,1)S(1)}, bf16[1,256]{1,0:T(2,128)(2,1)S(1)}, u32[]{:S(2)}, u32[]{:S(2)}) collective-permute-start(bf16[1,256]{1,0:T(2,128)(2,1)S(1)} %get-tuple-element.15), channel_id=1, source_target_pairs={{0,4},{4,8},{8,12},{12,16},{16,20},{20,24},{24,28},{1,5},{5,9},{9,... | collective-permute-start | bytes 1544 | tf_op jit(solution)/shard_map/ppermute | solution.py:17
  260.5 5.6 %copy-start.12 = (bf16[128,256]{1,0:T(8,128)(2,1)S(1)}, bf16[128,256]{1,0:T(8,128)(2,1)}, u32[]{:S(2)}) copy-start(bf16[128,256]{1,0:T(8,128)(2,1)} %param.21) | copy-start | bytes 196612
  260.5 6.3 %copy-start.13 = (bf16[128,256]{1,0:T(8,128)(2,1)S(1)}, bf16[128,256]{1,0:T(8,128)(2,1)}, u32[]{:S(2)}) copy-start(bf16[128,256]{1,0:T(8,128)(2,1)} %param.22) | copy-start | bytes 196612
  260.5 5.6 %collective-permute-start.1 = (bf16[1,256]{1,0:T(2,128)(2,1)S(1)}, bf16[1,256]{1,0:T(2,128)(2,1)S(1)}, u32[]{:S(2)}, u32[]{:S(2)}) collective-permute-start(bf16[1,256]{1,0:T(2,128)(2,1)S(1)} %get-tuple-element.16), channel_id=1, source_target_pairs={{4,0},{8,4},{12,8},{16,12},{20,16},{24,20},{28,24},{5,1},{9,5},{13... | collective-permute-start | bytes 1544 | tf_op jit(solution)/shard_map/ppermute | solution.py:19
Sparse Core Ops, SparseCore 0:
  169.5 33.3 reduce-scatter.2
  250.2 67.4 reduce-scatter.4
where the time goes:
time: 326 us; the launch traced here: 325 us
  blocking collectives  135 us (41%)
  waiting for transfers between devices  102 us (31%)
  local copies, waits for them, and re-layouts  25.9 us (8%)
  matrix products  21.7 us (7%)
  other arithmetic  15.7 us (5%)
  between operations  14.4 us (4%)
  starting transfers between devices  10.4 us (3%)
    all_to_all x1, blocking collectives, per_device(): lax.all_to_all(doubled, 'sp', split_axis=1, concat_axis=1, tiled=True)  123 us
    reduce_scatter x1, waiting for transfers between devices, per_device(): lax.psum_scatter(lax.dot_general(grad_resid, mixed, (((0,), (0,)), ((), (...  50.2 us
    reduce_scatter x1, waiting for transfers between devices, per_device(): lax.psum_scatter(partial_value, 'tp', scatter_dimension=2, tiled=True)  33.5 us
    all_to_all x1, waiting for transfers between devices, per_device(): lax.all_to_all(summed.astype(jnp.bfloat16), 'sp', split_axis=0, concat_ax...  17.1 us
    all_gather x1, blocking collectives, per_device(): grad_resid = lax.all_gather(resid_part, 'tp', axis=1, tiled=True)  6.76 us
  transfers between devices with their start and end apart: 5, of which 4 were waited for; matrix products, arithmetic and copies ran while one was open for 4% of the time, Pallas kernels for 0%

commit v1 on v0

--- a/solution.py
+++ b/solution.py
@@ -1,6 +1,10 @@
+import functools
+
 import jax
 import jax.numpy as jnp
 from jax import lax
+from jax.experimental import pallas as pl
+from jax.experimental.pallas import tpu as pltpu
 from jax.sharding import PartitionSpec as P
 
 epsilon = 1e-06
@@ -23,7 +27,7 @@
     return cells
 
 
-def per_device(
+def per_device_general(
     out_grad,
     residual,
     routes,
@@ -155,6 +159,423 @@
     )
 
 
+MESH = pl.DeviceIdType.MESH
+BF16 = jnp.bfloat16
+F32 = jnp.float32
+VMEM_LIMIT = 60 * 1024 * 1024
+
+
+def place():
+    sp, tp = lax.axis_index("sp"), lax.axis_index("tp")
+    return sp, tp, lax.div(sp, 2), lax.rem(sp, 2), lax.div(tp, 2), lax.rem(tp, 2)
+
+
+def greet(peers):
+    barrier = pltpu.get_barrier_semaphore()
+    for peer in peers:
+        pl.semaphore_signal(barrier, inc=1, device_id=peer, device_id_type=MESH)
+    return lambda: pl.semaphore_wait(barrier, len(peers))
+
+
+def columns_of(index, width):
+    return pl.ds(pl.multiple_of(index * width, width), width)
+
+
+def rows_of(index, height):
+    return pl.ds(pl.multiple_of(index * height, height), height)
+
+
+def dispatch_kernel(
+    slices, cap, rt, rw, resid, og, ogate, cout,
+    rows, grads, mixed, sel,
+    send_rows, send_grads, send_sem, recv_sem, local_sem,
+):
+    sp, tp, z, y, x, c = place()
+    pairs = slices // 2
+    tok, features = resid.shape
+    width = features // 4
+    sibling = (sp, 2 * x + 1 - c)
+    x_peer = (sp, 2 * (1 - x) + c)
+    y_peer = (2 * z + 1 - y, tp)
+    sp_peers = [(lax.rem(sp + k, slices), tp) for k in range(1, slices)]
+    ready = greet(sp_peers + [sibling, x_peer])
+
+    grid_r = lax.broadcasted_iota(jnp.int32, (tok, tok), 0)
+    grid_c = lax.broadcasted_iota(jnp.int32, (tok, tok), 1)
+    earlier = (grid_r < grid_c).astype(F32).astype(BF16)
+    slot = lax.broadcasted_iota(jnp.int32, (cap, tok), 0).astype(F32)
+    r32 = resid[...].astype(F32)
+    inv_rms = lax.rsqrt(jnp.mean(r32 * r32, axis=-1, keepdims=True) + epsilon)
+    mine = columns_of(tp, width)
+    normed = (resid[:, mine].astype(F32) * inv_rms).astype(BF16)
+    cot = og[:, mine]
+    for e in range(pairs):
+        named = (rt[...] == e).astype(F32)
+        mask = jnp.sum(named, axis=0, keepdims=True)
+        weight = jnp.sum(named * rw[...], axis=0, keepdims=True)
+        rank = jnp.dot(
+            jnp.broadcast_to(mask, (8, tok)).astype(BF16), earlier, preferred_element_type=F32
+        )[0:1]
+        pick = jnp.where((rank == slot) & (mask > 0.5), 1.0, 0.0)
+        slot_weight = jnp.sum(pick * weight, axis=1, keepdims=True)
+        pick = pick.astype(BF16)
+        here = slice(e * cap, (e + 1) * cap)
+        sel[here, :] = pick
+        send_rows[here, :] = jnp.dot(pick, normed, preferred_element_type=F32).astype(BF16)
+        send_grads[here, :] = (
+            slot_weight * jnp.dot(pick, cot, preferred_element_type=F32)
+        ).astype(BF16)
+    mixed[rows_of(sp, tok), :] = (ogate[...].astype(F32) * cout[...].astype(F32)).astype(BF16)
+    ready()
+
+    started = []
+
+    def send(n, src, dst, peer):
+        copy = pltpu.make_async_remote_copy(
+            src_ref=src, dst_ref=dst, send_sem=send_sem.at[n], recv_sem=recv_sem.at[n],
+            device_id=peer, device_id_type=MESH,
+        )
+        copy.start()
+        started.append(copy)
+        return copy
+
+    ours = ((send_rows, rows), (send_grads, grads))
+
+    def block(pair, yy, xx, cc):
+        return (rows_of(2 * pair + yy, cap), columns_of(2 * xx + cc, width))
+
+    arriving = {}
+    home = block(z, y, x, c)
+    for k in range(1, pairs):
+        far = lax.rem(z - k + pairs, pairs)
+        for a, (src, dst) in enumerate(ours):
+            arriving[k, a] = send(
+                16 * pairs + 2 * k + a, src.at[rows_of(far, cap), :], dst.at[home],
+                (2 * far + y, tp),
+            )
+    locals_ = []
+    for a, (src, dst) in enumerate(ours):
+        copy = pltpu.make_async_copy(src.at[rows_of(z, cap), :], dst.at[home], local_sem.at[a])
+        copy.start()
+        locals_.append(copy)
+    for copy in locals_:
+        copy.wait()
+
+    def spread(k):
+        pair = lax.rem(z + k, pairs)
+        at = block(pair, y, x, c)
+        out = {}
+        for a, (_, dst) in enumerate(ours):
+            out["x", a] = send(16 * k + a, dst.at[at], dst.at[at], x_peer)
+            out["y", a] = send(16 * k + 2 + a, dst.at[at], dst.at[at], y_peer)
+        for a, (_, dst) in enumerate(ours):
+            out["s", a] = send(16 * k + 4 + a, dst.at[at], dst.at[at], sibling)
+        return out
+
+    def forward(k, out):
+        pair = lax.rem(z + k, pairs)
+        got_x = block(pair, y, 1 - x, c)
+        got_y = block(pair, 1 - y, x, c)
+        out["x", 0].wait_recv()
+        out["dy"] = send(16 * k + 6, rows.at[got_x], rows.at[got_x], y_peer)
+        out["y", 1].wait_recv()
+        out["dx"] = send(16 * k + 7, grads.at[got_y], grads.at[got_y], x_peer)
+        out["x", 1].wait_recv()
+        out["y", 0].wait_recv()
+        for a, (_, dst) in enumerate(ours):
+            out["sx", a] = send(16 * k + 8 + a, dst.at[got_x], dst.at[got_x], sibling)
+            out["sy", a] = send(16 * k + 10 + a, dst.at[got_y], dst.at[got_y], sibling)
+
+    def finish(k, out):
+        pair = lax.rem(z + k, pairs)
+        got = block(pair, 1 - y, 1 - x, c)
+        out["dy"].wait_recv()
+        out["sd", 0] = send(16 * k + 12, rows.at[got], rows.at[got], sibling)
+        out["dx"].wait_recv()
+        out["sd", 1] = send(16 * k + 13, grads.at[got], grads.at[got], sibling)
+
+    outs = []
+    for k in range(pairs):
+        if k:
+            for a in range(2):
+                arriving[k, a].wait_recv()
+        outs.append(spread(k))
+        if k == pairs - 1:
+            mixed_copies = [
+                send(
+                    18 * pairs + j, mixed.at[rows_of(sp, tok), :], mixed.at[rows_of(sp, tok), :],
+                    peer,
+                )
+                for j, peer in enumerate(sp_peers)
+            ]
+        if k:
+            forward(k - 1, outs[k - 1])
+        if k > 1:
+            finish(k - 2, outs[k - 2])
+    forward(pairs - 1, outs[-1])
+    finish(pairs - 2, outs[-2])
+    finish(pairs - 1, outs[-1])
+    for out in outs:
+        for kind in ("s", "sx", "sy", "sd"):
+            for a in range(2):
+                out[kind, a].wait_recv()
+    for copy in mixed_copies:
+        copy.wait_recv()
+    for copy in started:
+        copy.wait_send()
+
+
+def dispatch(slices, cap, rt, rw, resid, og, ogate, cout):
+    features, tok = resid.shape[1], resid.shape[0]
+    pairs = slices // 2
+    vmem = pl.BlockSpec(memory_space=pltpu.VMEM)
+    sems = 18 * pairs + slices
+    return pl.pallas_call(
+        functools.partial(dispatch_kernel, slices, cap),
+        out_shape=(
+            jax.ShapeDtypeStruct((slices * cap, features), BF16),
+            jax.ShapeDtypeStruct((slices * cap, features), BF16),
+            jax.ShapeDtypeStruct((slices * tok, ogate.shape[1]), BF16),
+            jax.ShapeDtypeStruct((pairs * cap, tok), BF16),
+        ),
+        in_specs=[vmem] * 6,
+        out_specs=[vmem] * 4,
+        scratch_shapes=[
+            pltpu.VMEM((pairs * cap, features // 4), BF16),
+            pltpu.VMEM((pairs * cap, features // 4), BF16),
+            pltpu.SemaphoreType.DMA((sems,)),
+            pltpu.SemaphoreType.DMA((sems,)),
+            pltpu.SemaphoreType.DMA((2,)),
+        ],
+        compiler_params=pltpu.CompilerParams(
+            collective_id=0, has_side_effects=True, vmem_limit_bytes=VMEM_LIMIT
+        ),
+        name="dispatch",
+    )(rt, rw, resid, og, ogate, cout)
+
+
+def tail_kernel(
+    slices, cap, part, sel, resid, og, ogate, igate, cin, cout, taps, wout, mixed,
+    gresid, gogate, gigate, gcin, gwout,
+    sib, pairsum, plane, zsend, ret, dnq, dn, grx, edge_out, edge_in, send_sem, recv_sem,
+):
+    sp, tp, z, y, x, c = place()
+    pairs = slices // 2
+    tok, features = resid.shape
+    width = features // 4
+    sibling = (sp, 2 * x + 1 - c)
+    x_peer = (sp, 2 * (1 - x) + c)
+    x_other = (sp, 2 * (1 - x) + 1 - c)
+    y_peer = (2 * z + 1 - y, tp)
+    diagonal = (2 * z + 1 - y, 2 * (1 - x) + c)
+    sp_peers = [(lax.rem(sp + k, slices), tp) for k in range(1, slices)]
+    greet(sp_peers + [sibling, x_peer, x_other, diagonal])()
+    started = []
+
+    def send(n, src, dst, peer):
+        copy = pltpu.make_async_remote_copy(
+            src_ref=src, dst_ref=dst, send_sem=send_sem.at[n], recv_sem=recv_sem.at[n],
+            device_id=peer, device_id_type=MESH,
+        )
+        copy.start()
+        started.append(copy)
+        return copy
+
+    order = list(range(1, pairs)) + [0]
+    halves = {}
+    for k in order:
+        at = rows_of(lax.rem(z + k, pairs), 2 * cap)
+        for h in range(2):
+            halves[k, h] = send(
+                8 * k + h, part.at[at, columns_of(2 * h + 1 - c, width)], sib.at[h, at, :], sibling
+            )
+    moved = {}
+    for k in order:
+        pair = lax.rem(z + k, pairs)
+        at = rows_of(pair, 2 * cap)
+        for h in range(2):
+            halves[k, h].wait_recv()
+            pairsum[h, at, :] = (
+                part[at, columns_of(2 * h + c, width)].astype(F32) + sib[h, at, :].astype(F32)
+            ).astype(BF16)
+        same, other = rows_of(2 * pair + y, cap), rows_of(2 * pair + 1 - y, cap)
+        slots = rows_of(pair, cap)
+        moved[k] = [
+            send(8 * k + 2, pairsum.at[1 - x, same, :], plane.at[0, slots, :], x_peer),
+            send(8 * k + 3, pairsum.at[x, other, :], plane.at[1, slots, :], y_peer),
+            send(8 * k + 4, pairsum.at[1 - x, other, :], plane.at[2, slots, :], diagonal),
+        ]
+    back = []
+    for k in order:
+        pair = lax.rem(z + k, pairs)
+        slots = rows_of(pair, cap)
+        for copy in moved[k]:
+            copy.wait_recv()
+        total = (
+            pairsum[x, rows_of(2 * pair + y, cap), :].astype(F32)
+            + plane[0, slots, :].astype(F32)
+            + plane[1, slots, :].astype(F32)
+            + plane[2, slots, :].astype(F32)
+        ).astype(BF16)
+        if k:
+            zsend[slots, :] = total
+            back.append(
+                send(8 * k + 5, zsend.at[slots, :], ret.at[rows_of(z, cap), :], (2 * pair + y, tp))
+            )
+        else:
+            ret[slots, :] = total
+    r32 = resid[...].astype(F32)
+    inv_rms = lax.rsqrt(jnp.mean(r32 * r32, axis=-1, keepdims=True) + epsilon)
+    for copy in back:
+        copy.wait_recv()
+    first = 8 * pairs
+    quarter = lax.dot_general(
+        sel[...], ret[...], (((0,), (0,)), ((), ())), preferred_element_type=F32
+    ).astype(BF16)
+    dnq[...] = quarter
+    mine = columns_of(tp, width)
+    dn[:, mine] = quarter
+    shares = [
+        send(first + n, dnq, dn.at[:, mine], peer)
+        for n, peer in enumerate((x_other, x_peer, sibling))
+    ]
+    for copy in shares:
+        copy.wait_recv()
+    unit = r32 * inv_rms
+    d_normed = dn[...].astype(F32)
+    row_mean = jnp.mean(unit * d_normed, axis=-1, keepdims=True)
+    gresid[...] = (og[...].astype(F32) + inv_rms * (d_normed - unit * row_mean)).astype(BF16)
+    share = features // slices
+    first += 3
+    across = [
+        send(
+            first + n, gresid.at[:, columns_of(peer[0], share)], grx.at[rows_of(sp, tok), :], peer
+        )
+        for n, peer in enumerate(sp_peers)
+    ]
+    d_mix = lax.dot_general(
+        gresid[...], wout[...], (((1,), (1,)), ((), ())), preferred_element_type=F32
+    )
+    conv = cout[...].astype(F32)
+    d_conv = d_mix * ogate[...].astype(F32)
+    edge_out[0] = d_conv[tok - 8 :]
+    edge_out[1] = d_conv[:8]
+    first += slices
+    edges = [
+        send(first, edge_out.at[0], edge_in.at[0], sp_peers[0]),
+        send(first + 1, edge_out.at[1], edge_in.at[1], sp_peers[-1]),
+    ]
+    grx[rows_of(sp, tok), :] = gresid[:, columns_of(sp, share)]
+    gogate[...] = (d_mix * conv).astype(BF16)
+    for copy in edges:
+        copy.wait_recv()
+    before = jnp.where(sp > 0, edge_in[0, 7:8, :], 0.0)
+    after = jnp.where(sp < slices - 1, edge_in[1, 0:1, :], 0.0)
+    at = lax.broadcasted_iota(jnp.int32, d_conv.shape, 0)
+    later = jnp.where(at == tok - 1, after, pltpu.roll(d_conv, tok - 1, 0))
+    former = jnp.where(at == 0, before, pltpu.roll(d_conv, 1, 0))
+    d_inner = taps[0:1, :] * later + taps[1:2, :] * d_conv + taps[2:3, :] * former
+    gigate[...] = (d_inner * cin[...].astype(F32)).astype(BF16)
+    gcin[...] = (d_inner * igate[...].astype(F32)).astype(BF16)
+    for copy in across:
+        copy.wait_recv()
+    gwout[...] = lax.dot_general(
+        grx[...], mixed[...], (((0,), (0,)), ((), ())), preferred_element_type=F32
+    )
+    for copy in started:
+        copy.wait_send()
+
+
+def tail(slices, cap, part, sel, resid, og, ogate, igate, cin, cout, taps, wout, mixed):
+    tok, features = resid.shape
+    channels = ogate.shape[1]
+    pairs = slices // 2
+    width = features // 4
+    vmem = pl.BlockSpec(memory_space=pltpu.VMEM)
+    sems = 8 * pairs + 3 + slices + 2
+    small = jax.ShapeDtypeStruct((tok, channels), BF16)
+    return pl.pallas_call(
+        functools.partial(tail_kernel, slices, cap),
+        out_shape=(
+            jax.ShapeDtypeStruct((tok, features), BF16), small, small, small,
+            jax.ShapeDtypeStruct((features // slices, channels), F32),
+        ),
+        in_specs=[vmem] * 11,
+        out_specs=[vmem] * 5,
+        scratch_shapes=[
+            pltpu.VMEM((2, slices * cap, width), BF16),
+            pltpu.VMEM((2, slices * cap, width), BF16),
+            pltpu.VMEM((3, pairs * cap, width), BF16),
+            pltpu.VMEM((pairs * cap, width), BF16),
+            pltpu.VMEM((pairs * cap, width), BF16),
+            pltpu.VMEM((tok, width), BF16),
+            pltpu.VMEM((tok, features), BF16),
+            pltpu.VMEM((slices * tok, features // slices), BF16),
+            pltpu.VMEM((2, 8, channels), F32),
+            pltpu.VMEM((2, 8, channels), F32),
+            pltpu.SemaphoreType.DMA((sems,)),
+            pltpu.SemaphoreType.DMA((sems,)),
+        ],
+        compiler_params=pltpu.CompilerParams(
+            collective_id=1, has_side_effects=True, vmem_limit_bytes=VMEM_LIMIT
+        ),
+        name="tail",
+    )(part, sel, resid, og, ogate, igate, cin, cout, taps, wout, mixed)
+
+
+def per_device(
+    out_grad, residual, routes, route_weights, w_gate, w_up, w_down,
+    out_gate, in_gate, conv_input, conv_out, conv_taps, w_out,
+):
+    slices = lax.axis_size("sp")
+    cap = 5 * out_grad.shape[0] // slices
+    expert_rows, expert_grads, mixed, sel = dispatch(
+        slices, cap, routes.T, route_weights.T, residual, out_grad, out_gate, conv_out
+    )
+    gate_local, up_local, down_local = w_gate[0], w_up[0], w_down[0]
+    pre_gate = jnp.dot(expert_rows, gate_local, preferred_element_type=F32)
+    pre_up = jnp.dot(expert_rows, up_local, preferred_element_type=F32)
+    sigmoid_gate = jax.nn.sigmoid(pre_gate)
+    activated = pre_gate * sigmoid_gate
+    hidden = (activated * pre_up).astype(BF16)
+    d_hidden = lax.dot_general(
+        expert_grads, down_local, (((1,), (1,)), ((), ())), preferred_element_type=F32
+    )
+    grad_down = lax.dot_general(
+        hidden, expert_grads, (((0,), (0,)), ((), ())), preferred_element_type=F32
+    ).astype(BF16)
+    d_gate = (d_hidden * pre_up * sigmoid_gate * (1.0 + pre_gate * (1.0 - sigmoid_gate))).astype(
+        BF16
+    )
+    d_up = (d_hidden * activated).astype(BF16)
+    grad_up = lax.dot_general(
+        expert_rows, d_up, (((0,), (0,)), ((), ())), preferred_element_type=F32
+    ).astype(BF16)
+    partial_value = lax.dot_general(
+        d_gate, gate_local, (((1,), (1,)), ((), ())), preferred_element_type=F32
+    ) + lax.dot_general(d_up, up_local, (((1,), (1,)), ((), ())), preferred_element_type=F32)
+    grad_resid, grad_out_gate, grad_in_gate, grad_conv_input, grad_w_out = tail(
+        slices, cap, partial_value.astype(BF16), sel, residual, out_grad, out_gate, in_gate,
+        conv_input, conv_out, conv_taps, w_out, mixed,
+    )
+    return (
+        grad_resid, grad_up[None], grad_down[None], grad_out_gate, grad_in_gate,
+        grad_conv_input, grad_w_out,
+    )
+
+
+def fits_kernels(mesh, tokens):
+    slices = mesh.shape["sp"]
+    rows = tokens // slices
+    return mesh.shape["tp"] == 4 and slices >= 4 and (5 * rows // slices) % 16 == 0
+
+
+def on_device(mesh, out_grad, *rest):
+    tokens = out_grad.shape[0] * mesh.shape["sp"]
+    body = per_device if fits_kernels(mesh, tokens) else per_device_general
+    return body(out_grad, *rest)
+
+
 def solution(mesh):
     in_specs = (
         P("sp", None),
@@ -181,5 +602,5 @@
         P("sp", "tp"),
     )
     return jax.shard_map(
-        per_device, mesh=mesh, in_specs=in_specs, out_specs=out_specs, check_vma=False
-    )
+        functools.partial(on_device, mesh), mesh=mesh, in_specs=in_specs, out_specs=out_specs, check_vma=False
+    )

time: 326 us -> 119 us (0.37)
  blocking collectives: 135 us -> 0 us
  waiting for transfers between devices: 102 us -> 0 us
  Pallas kernels: 0 us -> 91.5 us
  local copies, waits for them, and re-layouts: 25.9 us -> 8.84 us
  other arithmetic: 15.7 us -> 0 us
  between operations: 14.4 us -> 0.73 us
  starting transfers between devices: 10.4 us -> 0 us
  matrix products: 21.7 us -> 18.1 us
    all_to_all x1 -> x0, blocking collectives: 123 us -> none  [per_device(): lax.all_to_all(doubled, 'sp', split_axis=1, concat_axis=1, tiled=True)]
    pallas_call x0 -> x2, Pallas kernels: none -> 91.5 us  [the longest x1 46.2 us: dispatch(): pl.pallas_call(functools.partial(dispatch_kernel, slices, cap), out_shape...]
    reduce_scatter x2 -> x0, waiting for transfers between devices: 83.7 us -> none  [the longest x1 50.2 us: per_device(): lax.psum_scatter(lax.dot_general(grad_resid, mixed, (((0,), (0,)), ((), (...]
    all_to_all x1 -> x0, waiting for transfers between devices: 17.1 us -> none  [per_device(): lax.all_to_all(summed.astype(jnp.bfloat16), 'sp', split_axis=0, concat_ax...]
    gather x4 -> x0, local copies, waits for them, and re-layouts: 9.04 us -> none  [the longest x1 3.02 us: per_device(): weighted[safe_index]]
    all_gather x1 -> x0, blocking collectives: 6.76 us -> none  [per_device(): grad_resid = lax.all_gather(resid_part, 'tp', axis=1, tiled=True)]
    mul x7 -> x0, local copies, waits for them, and re-layouts: 6.66 us -> none  [the longest x3 6.16 us: per_device(): route_weights[:, :, None] * out_grad.astype(jnp.float32)[:, None, :]]
    psum x1 -> x0, blocking collectives: 5.92 us -> none  [per_device(): row_dots = lax.psum(jnp.sum(unit_part * d_normed, axis=-1), 'tp')]
  transfers between devices with their start and end apart: 5 -> 0, of which waited for: 4 -> 0; matrix products, arithmetic and copies ran while one was open for 4% -> 0% of each run, Pallas kernels for 0% -> 0%
where the time goes in v1:
time: 119 us
  Pallas kernels  91.5 us (77%)
  matrix products  18.1 us (15%)
  local copies, waits for them, and re-layouts  8.84 us (7%)
    pallas_call x1, Pallas kernels, dispatch(): pl.pallas_call(functools.partial(dispatch_kernel, slices, cap), out_shape...  46.2 us
    pallas_call x1, Pallas kernels, tail(): pl.pallas_call(functools.partial(tail_kernel, slices, cap), out_shape=(ja...  45.3 us
    unnamed x15, local copies, waits for them, and re-layouts  8.84 us
    dot_general x1, matrix products, per_device(): pre_gate = jnp.dot(expert_rows, gate_local, preferred_element_type=F32)  3.4 us
    dot_general x1, matrix products, per_device(): lax.dot_general(hidden, expert_grads, (((0,), (0,)), ((), ())), preferred...  3.28 us
    dot_general x1, matrix products, per_device(): lax.dot_general(expert_rows, d_up, (((0,), (0,)), ((), ())), preferred_el...  3.17 us
    dot_general x1, matrix products, per_device(): lax.dot_general(d_up, up_local, (((1,), (1,)), ((), ())), preferred_eleme...  3.08 us

profile of v1, /device:TPU:0, one launch (start us, length us, event | category | flops | bytes accessed | tf_op | source)
XLA Modules:
  0.0 119.1 jit_solution(16730248533626846898)
XLA Ops:
  0.6 0.0 copy-start
  0.6 46.2 %dispatch.1 = (bf16[640,2048]{1,0:T(8,128)(2,1)}, bf16[640,2048]{1,0:T(8,128)(2,1)}, bf16[1024,256]{1,0:T(8,128)(2,1)}, bf16[320,128]{1,0:T(8,128)(2,1)}) custom-call(s32[2,128]{1,0:T(2,128)} %bitcast.28, f32[2,128]{1,0:T(2,128)} %bitcast.29, bf16[128,2048]{1,0:T(8,128)(2,1)} %resid.3, bf16[128,2048]{1,0:T(8,128)(2,1)} %og.3, bf16[128,256]{1,0:T(8,128)(2,1)} %ogate.3, ...), custom_call_target="tpu_custom_call" | custom-call | tf_op jit(solution)/shard_map/dispatch/pallas_call | solution.py:333
  46.9 0.0 copy-done
  46.9 0.0 copy-start.1
  46.9 0.0 copy-start.2
  46.9 3.4 %fusion.4 = f32[640,512]{1,0:T(8,128)S(1)} fusion(bf16[640,2048]{1,0:T(8,128)(2,1)} %get-tuple-element.17, bf16[1,2048,512]{2,1,0:T(8,128)(2,1)S(1)} %copy-done), kind=kOutput, calls=%fused_computation.7 | convolution fusion | flops 1342177280 | bytes 6029312 | tf_op jit(solution)/shard_map/dot_general | solution.py:536
  50.3 0.0 copy-done.1
  50.3 0.0 copy-done.2
  50.3 0.0 copy-start.3
  50.3 0.0 copy-start.4
  50.3 1.5 %fusion.7 = f32[640,512]{1,0:T(8,128)S(1)} fusion(bf16[640,2048]{1,0:T(8,128)(2,1)S(1)} %copy-done.2, bf16[1,2048,512]{2,1,0:T(8,128)(2,1)S(1)} %copy-done.1), kind=kOutput, calls=%fused_computation.10 | convolution fusion | flops 1342177280 | bytes 6029312 | tf_op jit(solution)/shard_map/dot_general | solution.py:537
  51.9 0.2 copy-done.3
  52.1 0.6 copy-done.4
  52.7 1.7 %multiply_convert_fusion.1 = (bf16[640,512]{1,0:T(8,128)(2,1)S(1)}, f32[640,512]{1,0:T(8,128)S(1)}) fusion(f32[640,512]{1,0:T(8,128)S(1)} %fusion.4, bf16[640,2048]{1,0:T(8,128)(2,1)S(1)} %copy-done.3, bf16[1,512,2048]{2,1,0:T(8,128)(2,1)S(1)} %copy-done.4), kind=kOutput, calls=%fused_computation.15 | convolution fusion | flops 1344143360 | bytes 7995392 | tf_op jit(solution)/shard_map/dot_general | solution.py:541
  54.4 3.3 %fusion.1 = bf16[1,512,2048]{2,1,0:T(8,128)(2,1)} fusion(bf16[640,2048]{1,0:T(8,128)(2,1)S(1)} %copy-done.3, f32[640,512]{1,0:T(8,128)S(1)} %fusion.7, f32[640,512]{1,0:T(8,128)S(1)} %fusion.4), kind=kOutput, calls=%fused_computation.4 | convolution fusion | flops 1345191936 | bytes 7340032 | tf_op jit(solution)/shard_map/dot_general | solution.py:544
  57.7 3.2 %fusion = bf16[1,2048,512]{2,1,0:T(8,128)(2,1)} fusion(bf16[640,2048]{1,0:T(8,128)(2,1)S(1)} %copy-done.2, bf16[640,512]{1,0:T(8,128)(2,1)S(1)} %get-tuple-element.25), kind=kOutput, calls=%fused_computation.3 | convolution fusion | flops 1343225856 | bytes 5373952 | tf_op jit(solution)/shard_map/dot_general | solution.py:551
  60.9 1.9 %fusion.2 = f32[640,2048]{1,0:T(8,128)S(1)} fusion(bf16[1,2048,512]{2,1,0:T(8,128)(2,1)S(1)} %copy-done, f32[640,512]{1,0:T(8,128)S(1)} %fusion.4, f32[640,512]{1,0:T(8,128)S(1)} %get-tuple-element.26, f32[640,512]{1,0:T(8,128)S(1)} %fusion.7), kind=kOutput, calls=%fused_computation.5 | convolution fusion | flops 1345454080 | bytes 11272192 | tf_op jit(solution)/shard_map/dot_general | solution.py:554
  62.8 3.1 %add_convert_fusion.part = bf16[640,2048]{1,0:T(8,128)(2,1)} fusion(f32[640,2048]{1,0:T(8,128)S(1)} %fusion.2, bf16[640,512]{1,0:T(8,128)(2,1)S(1)} %get-tuple-element.25, bf16[1,2048,512]{2,1,0:T(8,128)(2,1)S(1)} %copy-done.1), kind=kOutput, calls=%fused_computation | convolution fusion | flops 1344798720 | bytes 10616832 | tf_op jit(solution)/shard_map/dot_general | solution.py:556
  65.9 45.3 %tail.1 = (bf16[128,2048]{1,0:T(8,128)(2,1)}, bf16[128,256]{1,0:T(8,128)(2,1)}, bf16[128,256]{1,0:T(8,128)(2,1)}, bf16[128,256]{1,0:T(8,128)(2,1)}, f32[256,256]{1,0:T(8,128)}) custom-call(bf16[640,2048]{1,0:T(8,128)(2,1)} %add_convert_fusion.part, bf16[320,128]{1,0:T(8,128)(2,1)} %get-tuple-element.18.sel, bf16[128,2048]{1,0:T(8,128)(2,1)} %resid.3, ...), custom_call_target="tpu_custom_call" | custom-call | tf_op jit(solution)/shard_map/tail/pallas_call | solution.py:497
  111.2 1.9 %copy.25 = bf16[128,2048]{1,0:T(8,128)(2,1)} copy(bf16[128,2048]{1,0:T(8,128)(2,1)} %get-tuple-element.34) | data formatting | bytes 1048576
  113.0 1.5 %copy.26 = bf16[128,256]{1,0:T(8,128)(2,1)} copy(bf16[128,256]{1,0:T(8,128)(2,1)} %get-tuple-element.37) | data formatting | bytes 131072
  114.5 1.5 %copy.27 = bf16[128,256]{1,0:T(8,128)(2,1)} copy(bf16[128,256]{1,0:T(8,128)(2,1)} %get-tuple-element.38) | data formatting | bytes 131072
  116.0 1.5 %copy.28 = bf16[128,256]{1,0:T(8,128)(2,1)} copy(bf16[128,256]{1,0:T(8,128)(2,1)} %get-tuple-element.39) | data formatting | bytes 131072
  117.5 1.7 %copy.29 = f32[256,256]{1,0:T(8,128)} copy(f32[256,256]{1,0:T(8,128)} %get-tuple-element.40) | data formatting | bytes 524288
Async XLA Ops:
  0.6 46.2 %copy-start = (bf16[1,2048,512]{2,1,0:T(8,128)(2,1)S(1)}, bf16[1,2048,512]{2,1,0:T(8,128)(2,1)}, u32[]{:S(2)}) copy-start(bf16[1,2048,512]{2,1,0:T(8,128)(2,1)} %param.17) | copy-start | bytes 6291460
  46.9 3.4 %copy-start.1 = (bf16[1,2048,512]{2,1,0:T(8,128)(2,1)S(1)}, bf16[1,2048,512]{2,1,0:T(8,128)(2,1)}, u32[]{:S(2)}) copy-start(bf16[1,2048,512]{2,1,0:T(8,128)(2,1)} %param.18) | copy-start | bytes 6291460
  46.9 3.4 %copy-start.2 = (bf16[640,2048]{1,0:T(8,128)(2,1)S(1)}, bf16[640,2048]{1,0:T(8,128)(2,1)}, u32[]{:S(2)}) copy-start(bf16[640,2048]{1,0:T(8,128)(2,1)} %get-tuple-element.17) | copy-start | bytes 7864324
  50.3 1.7 %copy-start.3 = (bf16[640,2048]{1,0:T(8,128)(2,1)S(1)}, bf16[640,2048]{1,0:T(8,128)(2,1)}, u32[]{:S(2)}) copy-start(bf16[640,2048]{1,0:T(8,128)(2,1)} %get-tuple-element.16) | copy-start | bytes 7864324
  50.3 2.4 %copy-start.4 = (bf16[1,512,2048]{2,1,0:T(8,128)(2,1)S(1)}, bf16[1,512,2048]{2,1,0:T(8,128)(2,1)}, u32[]{:S(2)}) copy-start(bf16[1,512,2048]{2,1,0:T(8,128)(2,1)} %param.19) | copy-start | bytes 6291460
